TPU v7x, 32 devices: a whole 2x2x4 slice. The times are simulated.
32 devices in a mesh: rep: 2 (over x), fs: 8 (over z, y), tp: 2 (over core).
Axes of the slice: x: 2, y: 2, z: 4, core: 2. Of those that a mesh axis runs over, the one named last changes fastest.
Arguments:
- mixed_input: bfloat16 [8192, 1024], P(('rep', 'fs', 'tp')), may hold values from -6 to 6
- project_weight: bfloat16 [1024, 1024], P(('fs', 'tp')), may hold values from -0.1875 to 0.1875
- norm_gain: float32 [1024], replicated, may hold values from 0.1 to 1.9
- up_weight: bfloat16 [1024, 4096], P('fs', 'tp'), may hold values from -0.1875 to 0.1875
- down_weight: bfloat16 [4096, 1024], P('tp', 'fs'), may hold values from -0.09375 to 0.09375
Outputs:
- mlp_output: bfloat16 [8192, 1024], P(('rep', 'fs', 'tp'))
All inputs are finite; a program needn't handle non-finite values.
Results may differ from a plain program's by a relative error of at most 0.015.
Values may be sent and summed in bfloat16 or wider, within the bound.
A program may use at most 64 MiB of HBM per device.

v0:
```python
import jax
import jax.numpy as jnp
from jax import lax
from jax.sharding import PartitionSpec as P

epsilon = 1e-06


def gathered_then(section, axis, dim, apply):
    everything = lax.all_gather(section, axis, axis=dim, tiled=True)
    return apply(everything, jnp.int32(0))


def own_rows(contribution, width, axis):
    whole = contribution(jnp.int32(0), width * lax.axis_size(axis)).astype(jnp.bfloat16)
    return lax.psum_scatter(whole, axis, scatter_dimension=0, tiled=True).astype(jnp.float32)


def local(mixed_input, project_weight, norm_gain, up_weight, down_weight):
    whole_project = lax.all_gather(project_weight, ("fs", "tp"), axis=0, tiled=True)
    projected = jnp.dot(mixed_input, whole_project, preferred_element_type=jnp.float32).astype(
        jnp.bfloat16
    )
    values = projected.astype(jnp.float32)
    scale = lax.rsqrt(jnp.mean(values * values, axis=-1, keepdims=True) + epsilon)
    normed = (values * scale * norm_gain.astype(jnp.float32)).astype(jnp.bfloat16)
    up_full = lax.all_gather(up_weight, "fs", axis=0, tiled=True)
    down_full = lax.all_gather(down_weight, "fs", axis=1, tiled=True)

    def lifted(token_piece, first_row):
        preact = jnp.dot(token_piece, up_full, preferred_element_type=jnp.float32)
        return jnp.square(jax.nn.relu(preact)).astype(jnp.bfloat16)

    hidden = gathered_then(normed, "tp", 0, lifted)

    def partial_term(first_row, row_count):
        row_block = lax.dynamic_slice_in_dim(hidden, first_row, row_count, 0)
        return jnp.dot(row_block, down_full, preferred_element_type=jnp.float32)

    summed = own_rows(partial_term, mixed_input.shape[0], "tp")
    return summed.astype(jnp.bfloat16)


def solution(mesh):
    placed = (
        P(("rep", "fs", "tp"), None),
        P(("fs", "tp"), None),
        P(),
        P("fs", "tp"),
        P("tp", "fs"),
    )
    return jax.shard_map(
        local, mesh=mesh, in_specs=placed, out_specs=P(("rep", "fs", "tp"), None), check_vma=False
    )
```

profile of v0, /device:TPU:0, one launch (start us, length us, event | category | flops | bytes accessed | tf_op | source)
XLA Modules:
  0.0 239.8 jit_solution(3866611374542259978)
XLA Ops:
  6.5 0.0 copy-start
  6.5 0.0 all-gather.5.cloned.1.call-start
  6.5 0.7 all-gather.5.cloned.1.call-update
  7.3 0.0 all-gather.7.cloned.1.call-start
  7.3 46.7 %all-gather.5.cloned.1.call-done = bf16[1024,1024]{1,0:T(8,128)(2,1)} async-done(((bf16[64,1024]{1,0:T(8,128)(2,1)}), bf16[1024,1024]{1,0:T(8,128)(2,1)}) %all-gather.5.cloned.1.call-update) | async-done | bytes 2097168 | tf_op jit(solution)/shard_map/all_gather | solution.py:20
  54.0 0.0 copy-done
  54.0 2.4 fusion
  56.4 1.7 fusion.2
  58.1 0.0 all-gather.7.cloned.1.call-update
  58.1 0.0 all-gather.9.cloned.1.call-start
  58.2 0.7 all-gather.9.cloned.1.call-update
  58.9 0.0 all-gather.11.cloned.1.call-start
  58.9 0.5 all-gather.11.cloned.1.call-update
  59.5 0.0 reduce-scatter.2.cloned.1.call-start
  59.5 6.4 %all-gather.7.cloned.1.call-done = bf16[512,1024]{1,0:T(8,128)(2,1)} async-done(((bf16[256,1024]{1,0:T(8,128)(2,1)}), bf16[512,1024]{1,0:T(8,128)(2,1)}) %all-gather.7.cloned.1.call-update) | async-done | bytes 1048592 | tf_op jit(solution)/shard_map/all_gather | solution.py:10
  65.9 76.4 %all-gather.9.cloned.1.call-done = bf16[1024,2048]{1,0:T(8,128)(2,1)} async-done(((bf16[128,2048]{1,0:T(8,128)(2,1)}), bf16[1024,2048]{1,0:T(8,128)(2,1)}) %all-gather.9.cloned.1.call-update) | async-done | bytes 4194320 | tf_op jit(solution)/shard_map/all_gather | solution.py:27
  142.3 74.8 %all-gather.11.cloned.1.call-done = bf16[2048,1024]{1,0:T(8,128)(2,1)} async-done(((bf16[2048,128]{1,0:T(8,128)(2,1)}), bf16[2048,1024]{1,0:T(8,128)(2,1)}) %all-gather.11.cloned.1.call-update) | async-done | bytes 4194320 | tf_op jit(solution)/shard_map/all_gather | solution.py:28
  217.1 9.2 %convolution_convert_fusion = bf16[512,1024]{1,0:T(8,128)(2,1)} fusion(bf16[2048,1024]{1,0:T(8,128)(2,1)} %all-gather.11.cloned.1.call-done, bf16[512,1024]{1,0:T(8,128)(2,1)} %all-gather.7.cloned.1.call-done, bf16[1024,2048]{1,0:T(8,128)(2,1)} %all-gather.9.cloned.1.call-done), kind=kOutput, calls=%fused_computation.1 | convolution fusion | flops 4298637312 | bytes 10485760 | tf_op jit(solution)/shard_map/dot_general | solution.py:38
  226.3 0.0 reduce-scatter.2.cloned.1.call-update
  226.3 7.0 %reduce-scatter.2.cloned.1.call-done = bf16[256,1024]{1,0:T(8,128)(2,1)} async-done(((bf16[512,1024]{1,0:T(8,128)(2,1)}), bf16[256,1024]{1,0:T(8,128)(2,1)}) %reduce-scatter.2.cloned.1.call-update) | async-done | bytes 524304 | tf_op jit(solution)/shard_map/reduce_scatter | solution.py:16
  (1 shorter events, 0.0 us)
Async XLA Ops:
  6.5 47.5 %copy-start = (bf16[256,1024]{1,0:T(8,128)(2,1)S(1)}, bf16[256,1024]{1,0:T(8,128)(2,1)}, u32[]{:S(2)}) copy-start(bf16[256,1024]{1,0:T(8,128)(2,1)} %param.5) | copy-start | bytes 1572868
  6.5 47.5 %all-gather.5.cloned.1.call-start = ((), (), s32[]{:S(2)}) async-start(), calls=%async_computation.1 | async-start | bytes 2228224 | tf_op jit(solution)/shard_map/all_gather | solution.py:20
  7.3 58.6 %all-gather.7.cloned.1.call-start = ((), (), s32[]{:S(2)}) async-start(), calls=%async_computation.2 | async-start | bytes 1572864 | tf_op jit(solution)/shard_map/all_gather | solution.py:10
  58.1 84.2 %all-gather.9.cloned.1.call-start = ((), (), s32[]{:S(2)}) async-start(), calls=%async_computation.3 | async-start | bytes 4718592 | tf_op jit(solution)/shard_map/all_gather | solution.py:27
  58.9 158.2 %all-gather.11.cloned.1.call-start = ((), (), s32[]{:S(2)}) async-start(), calls=%async_computation.4 | async-start | bytes 4718592 | tf_op jit(solution)/shard_map/all_gather | solution.py:28
  59.5 173.8 %reduce-scatter.2.cloned.1.call-start = ((), (), s32[]{:S(2)}) async-start(), calls=%async_computation.5 | async-start | bytes 1572864 | tf_op jit(solution)/shard_map/reduce_scatter | solution.py:16
Sparse Core Ops, SparseCore 0:
  9.5 44.5 all-gather.4
  58.3 7.5 all-gather.6
  68.0 74.2 all-gather.8
  144.2 72.8 all-gather.10
  226.4 6.7 reduce-scatter.1
where the time goes:
time: 240 us
  waiting for transfers between devices  213 us (89%)
  between operations  13.1 us (5%)
  matrix products  11.6 us (5%)
    all_gather x1, waiting for transfers between devices, local(): up_full = lax.all_gather(up_weight, 'fs', axis=0, tiled=True)  76.4 us
    all_gather x1, waiting for transfers between devices, local(): down_full = lax.all_gather(down_weight, 'fs', axis=1, tiled=True)  74.8 us
    all_gather x1, waiting for transfers between devices, local(): lax.all_gather(project_weight, ('fs', 'tp'), axis=0, tiled=True)  46.7 us
    dot_general x1, matrix products, partial_term(): return jnp.dot(row_block, down_full, preferred_element_type=jnp.float32)  9.23 us
    reduce_scatter x1, waiting for transfers between devices, own_rows(): lax.psum_scatter(whole, axis, scatter_dimension=0, tiled=True)  6.96 us
    all_gather x1, waiting for transfers between devices, gathered_then(): everything = lax.all_gather(section, axis, axis=dim, tiled=True)  6.35 us
  transfers between devices with their start and end apart: 5, of which 5 were waited for; matrix products, arithmetic and copies ran while one was open for 0% of the time, Pallas kernels for 0%

commit v1 on v0

v1 whole, which is shorter than its diff:
```python
import functools

import jax
import jax.numpy as jnp
from jax import lax
from jax.experimental import pallas as pl
from jax.experimental.pallas import tpu as pltpu
from jax.sharding import PartitionSpec as P

epsilon = 1e-06
MESH = pl.DeviceIdType.MESH


def kernel(R, F, T, ring_project, mixed_ref, project_ref, gain_ref, up_ref, down_ref, out_ref,
           mixed, project, up, down, hidden, own, outgoing, incoming,
           local_sem, mix_send, mix_recv, ring_send, ring_recv, pass_send, pass_recv,
           sum_send, sum_recv):
    G = R * T
    half_ring = F // 2
    r, f, t = lax.axis_index("rep"), lax.axis_index("fs"), lax.axis_index("tp")
    at = f // 2 + lax.rem(f, 2) * (F - 1 - 2 * (f // 2))

    def shard_at(position):
        position = lax.rem(position + 2 * F, F)
        back = position // half_ring
        return 2 * position * (1 - back) + back * (2 * (F - 1 - position) + 1)

    neighbour = (shard_at(at + 1), shard_at(at - 1))

    def owner(direction, distance):
        return shard_at(at - distance) if direction == 0 else shard_at(at + distance)

    def peer(k):
        return {"rep": lax.rem(r + k // T, R), "fs": f, "tp": lax.rem(t + lax.rem(k, T), T)}

    def seen_from(k):
        return lax.rem(R - k // T, R) * T + lax.rem(T - lax.rem(k, T), T)

    width = hidden.shape[-1]
    first = pl.multiple_of(r * width, width)
    if ring_project:
        rows = project_ref.shape[0]
    up_rows = up_ref.shape[0]

    def slices(tensor, who, h):
        if tensor == 0:
            n = project.shape[1] // 2
            place = pl.ds(pl.multiple_of((who * T + t) * rows, rows), rows)
            cols = pl.ds(h * n, n)
            return project_ref.at[:, cols], project.at[place, cols]
        if tensor == 1:
            n = up_rows // 2
            place = pl.ds(pl.multiple_of(who * up_rows + h * n, n), n)
            return up_ref.at[pl.ds(h * n, n), pl.ds(first, width)], up.at[place, :]
        n = width // 2
        source = down_ref.at[pl.ds(pl.multiple_of(r * width + h * n, n), n), :]
        return source, down.at[who, pl.ds(h * n, n), :]

    def hop(tensor, direction, distance, h):
        given, slot = slices(tensor, owner(direction, distance - 1), h)
        index = ((tensor * 2 + direction) * half_ring + distance - 1) * 2 + h
        return pltpu.make_async_remote_copy(
            src_ref=given if distance == 1 else slot,
            dst_ref=slot,
            send_sem=ring_send.at[index],
            recv_sem=ring_recv.at[index],
            device_id={"rep": r, "fs": neighbour[direction], "tp": t},
            device_id_type=MESH,
        )

    def arrived(tensor, direction, distance, h):
        index = ((tensor * 2 + direction) * half_ring + distance - 1) * 2 + h
        given, slot = slices(tensor, owner(direction, distance), h)
        pltpu.make_async_remote_copy(
            src_ref=slot, dst_ref=slot, send_sem=ring_send.at[index],
            recv_sem=ring_recv.at[index],
            device_id={"rep": r, "fs": neighbour[direction], "tp": t}, device_id_type=MESH,
        ).wait_recv()

    def halves(direction, distance):
        return (0, 1) if distance < half_ring else (direction,)

    started = []

    def step(tensor, distance):
        for h in (0, 1):
            for direction in (0, 1):
                if distance > 1:
                    arrived(tensor, direction, distance - 1, h)
                if h in halves(direction, distance):
                    copy = hop(tensor, direction, distance, h)
                    copy.start()
                    started.append(copy)

    def last(tensor):
        for direction in (0, 1):
            for h in halves(direction, half_ring):
                arrived(tensor, direction, half_ring, h)

    def owners(distance):
        if distance == 0:
            return ((0, f),)
        if distance == half_ring:
            return ((0, owner(0, distance)),)
        return ((0, owner(0, distance)), (1, owner(1, distance)))

    barrier = pltpu.get_barrier_semaphore()
    for direction in (0, 1):
        pl.semaphore_signal(barrier, inc=1, device_id={"rep": r, "fs": neighbour[direction], "tp": t},
                            device_id_type=MESH)
    for k in range(1, G):
        pl.semaphore_signal(barrier, inc=1, device_id=peer(k), device_id_type=MESH)
    pl.semaphore_wait(barrier, 2 + G - 1)

    if ring_project:
        step(0, 1)
    mixes = []
    for k in range(1, G):
        there = (R - k // T) % R * T + (T - k % T) % T
        copy = pltpu.make_async_remote_copy(
            src_ref=mixed_ref, dst_ref=mixed.at[there], send_sem=mix_send.at[k],
            recv_sem=mix_recv.at[there], device_id=peer(k), device_id_type=MESH)
        copy.start()
        mixes.append(copy)

    passes = []

    def pass_on(distance):
        for _, who in owners(distance):
            for dt in range(1, T):
                number = len(passes)
                place = project.at[pl.ds(pl.multiple_of((who * T + t) * rows, rows), rows), :]
                copy = pltpu.make_async_remote_copy(
                    src_ref=project_ref if distance == 0 else place, dst_ref=place,
                    send_sem=pass_send.at[number], recv_sem=pass_recv.at[number],
                    device_id=peer(dt), device_id_type=MESH)
                copy.start()
                passes.append((copy, who, dt))

    locals_ = [pltpu.make_async_copy(mixed_ref, mixed.at[0], local_sem.at[0])]
    for h in (0, 1):
        for tensor in (0, 1, 2) if ring_project else (1, 2):
            given, slot = slices(tensor, f, h)
            locals_.append(pltpu.make_async_copy(given, slot, local_sem.at[1 + 2 * tensor + h]))
    if not ring_project:
        locals_.append(pltpu.make_async_copy(project_ref, project, local_sem.at[1]))
    for copy in locals_:
        copy.start()
    if ring_project:
        pass_on(0)
        for distance in range(2, half_ring + 1):
            step(0, distance)
            pass_on(distance - 1)

    step(1, 1)
    if ring_project:
        last(0)
        pass_on(half_ring)
    step(1, 2) if half_ring > 1 else None
    for copy in locals_:
        copy.wait()
    if ring_project:
        for copy, who, dt in passes:
            copy.wait_recv()

    def norm_block(k):
        values = jnp.dot(mixed[k], project[...], preferred_element_type=jnp.float32)
        values = values.astype(jnp.bfloat16).astype(jnp.float32)
        scale = lax.rsqrt(jnp.mean(values * values, axis=-1, keepdims=True) + epsilon)
        mixed[k] = (values * scale * gain_ref[...]).astype(jnp.bfloat16)

    def norm_peer(k, carry):
        pltpu.make_async_copy(mixed.at[k], mixed.at[k], mix_recv.at[k]).wait()
        norm_block(k)
        return carry

    norm_block(0)
    split = max(G // 2, 1)
    lax.fori_loop(1, split, norm_peer, 0)
    for distance in range(3, half_ring + 1):
        step(1, distance)
    step(2, 1)
    lax.fori_loop(split, G, norm_peer, 0)
    last(1)

    def lift(k, carry):
        preact = jnp.dot(mixed[k], up[...], preferred_element_type=jnp.float32)
        hidden[k] = jnp.square(jnp.maximum(preact, 0.0)).astype(jnp.bfloat16)
        return carry

    lax.fori_loop(0, G, lift, 0)

    def sum_copy(k, who):
        there = seen_from(k)
        return pltpu.make_async_remote_copy(
            src_ref=outgoing.at[k, who], dst_ref=incoming.at[there, who],
            send_sem=sum_send.at[k, who], recv_sem=sum_recv.at[there, who],
            device_id=peer(k), device_id_type=MESH)

    def lower(who):
        def one(i, carry):
            k = G - i
            part = jnp.dot(hidden[k], down[who], preferred_element_type=jnp.float32)
            outgoing[k, who] = part.astype(jnp.bfloat16)
            sum_copy(k, who).start()
            return carry

        lax.fori_loop(1, G, one, 0)
        own[who] = jnp.dot(hidden[0], down[who], preferred_element_type=jnp.float32)

    for distance in range(2, half_ring + 1):
        step(2, distance)
        for _, who in owners(distance - 2):
            lower(who)
    for _, who in owners(half_ring - 1):
        lower(who)
    last(2)
    for _, who in owners(half_ring):
        lower(who)

    def settle(k, carry):
        for j in range(F):
            copy = sum_copy(k, j)
            copy.wait_send()
            pltpu.make_async_copy(incoming.at[k, j], incoming.at[k, j], sum_recv.at[k, j]).wait()
        return carry

    lax.fori_loop(1, G, settle, 0)
    w = own.shape[-1]
    for j in range(F):
        total = own[j]
        for k in range(1, G):
            total += incoming[k, j].astype(jnp.float32)
        out_ref[:, j * w:(j + 1) * w] = total.astype(jnp.bfloat16)
    for copy in started + mixes + [p[0] for p in passes]:
        copy.wait_send()


def local(R, F, T, mixed_input, project_weight, norm_gain, up_weight, down_weight):
    G = R * T
    tokens, mix = mixed_input.shape
    width = up_weight.shape[1] // R
    cols = down_weight.shape[1]
    model = project_weight.shape[1]
    ring_project = project_weight.shape[0] % 16 == 0
    if not ring_project:
        project_weight = lax.all_gather(project_weight, ("fs", "tp"), axis=0, tiled=True)
    hops = 3 * 2 * (F // 2) * 2
    dma = pltpu.SemaphoreType.DMA
    flops = 2 * G * tokens * (mix * model + 2 * model * width)
    return pl.pallas_call(
        functools.partial(kernel, R, F, T, ring_project),
        out_shape=jax.ShapeDtypeStruct((tokens, model), jnp.bfloat16),
        in_specs=[pl.BlockSpec(memory_space=pltpu.VMEM)] * 5,
        out_specs=pl.BlockSpec(memory_space=pltpu.VMEM),
        scratch_shapes=[
            pltpu.VMEM((G, tokens, mix), jnp.bfloat16),
            pltpu.VMEM((mix, model), jnp.bfloat16),
            pltpu.VMEM((model, width), jnp.bfloat16),
            pltpu.VMEM((F, width, cols), jnp.bfloat16),
            pltpu.VMEM((G, tokens, width), jnp.bfloat16),
            pltpu.VMEM((F, tokens, cols), jnp.float32),
            pltpu.VMEM((G, F, tokens, cols), jnp.bfloat16),
            pltpu.VMEM((G, F, tokens, cols), jnp.bfloat16),
            dma((8,)),
            dma((G,)), dma((G,)),
            dma((hops,)), dma((hops,)),
            dma((F * max(T - 1, 1),)), dma((F * max(T - 1, 1),)),
            dma((G, F)), dma((G, F)),
        ],
        compiler_params=pltpu.CompilerParams(
            collective_id=0, has_side_effects=True, vmem_limit_bytes=60 * 2 ** 20),
        cost_estimate=pl.CostEstimate(flops=flops, bytes_accessed=4 * 2 ** 20, transcendentals=0),
    )(mixed_input, project_weight, norm_gain.astype(jnp.float32).reshape(1, -1), up_weight, down_weight)


def solution(mesh):
    placed = (
        P(("rep", "fs", "tp"), None),
        P(("fs", "tp"), None),
        P(),
        P("fs", "tp"),
        P("tp", "fs"),
    )
    body = functools.partial(local, *(mesh.shape[name] for name in ("rep", "fs", "tp")))
    return jax.shard_map(
        body, mesh=mesh, in_specs=placed, out_specs=P(("rep", "fs", "tp"), None), check_vma=False
    )
```

time: 240 us -> 77.8 us (0.32)
  waiting for transfers between devices: 213 us -> 0 us
  Pallas kernels: 0 us -> 75.8 us
  between operations: 13.1 us -> 0.01 us
  matrix products: 11.6 us -> 0 us
    all_gather x4 -> x0, waiting for transfers between devices: 204 us -> none  [the longest x1 76.4 us: local(): up_full = lax.all_gather(up_weight, 'fs', axis=0, tiled=True)]
    pallas_call x0 -> x1, Pallas kernels: none -> 75.8 us  [local(): pl.pallas_call(functools.partial(kernel, R, F, T, ring_project), out_shap...]
    dot_general x2 -> x0, matrix products: 11.6 us -> none  [the longest x1 9.23 us: partial_term(): return jnp.dot(row_block, down_full, preferred_element_type=jnp.float32)]
    reduce_scatter x1 -> x0, waiting for transfers between devices: 6.96 us -> none  [own_rows(): lax.psum_scatter(whole, axis, scatter_dimension=0, tiled=True)]
  transfers between devices with their start and end apart: 5 -> 0, of which waited for: 5 -> 0; matrix products, arithmetic and copies ran while one was open for 0% -> 0% of each run, Pallas kernels for 0% -> 0%
where the time goes in v1:
time: 77.8 us; the launch traced here: 77.7 us
  Pallas kernels  75.8 us (97%)
  local copies, waits for them, and re-layouts  1.87 us (2%)
    pallas_call x1, Pallas kernels, local(): pl.pallas_call(functools.partial(kernel, R, F, T, ring_project), out_shap...  75.8 us
    unnamed x1, local copies, waits for them, and re-layouts  1.87 us

profile of v1, /device:TPU:0, one launch (start us, length us, event | category | flops | bytes accessed | tf_op | source)
XLA Modules:
  0.0 77.7 jit_solution(17266710540997810066)
XLA Ops:
  0.0 75.8 %shard_map.55 = bf16[256,1024]{1,0:T(8,128)(2,1)} custom-call(bf16[256,1024]{1,0:T(8,128)(2,1)} %mixed_ref.1, bf16[64,1024]{1,0:T(8,128)(2,1)} %project_ref.1, f32[1,1024]{1,0:T(1,128)} %bitcast.1, bf16[128,2048]{1,0:T(8,128)(2,1)} %up_ref.1, bf16[2048,128]{1,0:T(8,128)(2,1)} %down_ref.1), custom_call_target="tpu_custom_call" | custom-call | flops 6442450944 | bytes 4194304 | tf_op jit(solution)/shard_map/pallas_call | solution.py:251
  75.8 1.9 %copy.7 = bf16[256,1024]{1,0:T(8,128)(2,1)} copy(bf16[256,1024]{1,0:T(8,128)(2,1)} %shard_map.55) | data formatting | bytes 1048576
